TPU v7x, 32 devices: a whole 2x2x4 slice. The times are simulated.
32 devices in a mesh: ep: 8 (over z, y), tp: 4 (over x, core).
Axes of the slice: x: 2, y: 2, z: 4, core: 2. Of those that a mesh axis runs over, the one named last changes fastest.
Arguments:
- tokens: bfloat16 [128, 2048], P('ep'), may hold values from -6 to 6
- head_state: float32 [128, 16, 4096], P('ep', 'tp'), may hold values from -6 to 6
- mixer_gain: float32 [2048], replicated, may hold values from 0.1 to 1.9
- w_query: bfloat16 [2048, 1024], P('ep', 'tp'), may hold values from -0.125 to 0.125
- w_key: bfloat16 [2048, 1024], P('ep', 'tp'), may hold values from -0.125 to 0.125
- w_value: bfloat16 [2048, 1024], P('ep', 'tp'), may hold values from -0.125 to 0.125
- decay_down: bfloat16 [2048, 64], replicated, may hold values from -0.125 to 0.125
- decay_up: bfloat16 [64, 1024], replicated, may hold values from -3 to 3
- decay_base: float32 [1024], P('tp'), may hold values from -4 to 0
- rate_down: bfloat16 [2048, 64], replicated, may hold values from -0.125 to 0.125
- rate_up: bfloat16 [64, 1024], replicated, may hold values from -0.75 to 0.75
- head_gain: float32 [1024], P('tp'), may hold values from 0.1 to 1.9
- w_out: bfloat16 [1024, 2048], P('tp', 'ep'), may hold values from -0.1875 to 0.1875
- expert_gain: float32 [2048], replicated, may hold values from 0.1 to 1.9
- expert_ids: int32 [128, 2], P('ep'), may hold values from 0 to 7, all different within a row; in each aligned block of 16 rows (0 to 15, 16 to 31, ...) at most 8 rows name the same one
- route_weight: float32 [128, 2], P('ep'), may hold values from 0.2 to 1
- w_gate: bfloat16 [8, 2048, 512], P('ep', None, 'tp'), may hold values from -0.125 to 0.125
- w_up: bfloat16 [8, 2048, 512], P('ep', None, 'tp'), may hold values from -0.125 to 0.125
- w_down: bfloat16 [8, 512, 2048], P('ep', 'tp'), may hold values from -0.25 to 0.25
Outputs:
- layer_out: bfloat16 [128, 2048], P('ep', 'tp')
- next_state: float32 [128, 16, 4096], P('ep', 'tp')
Inputs may be any that keep to these rules, and one draw needn't show every extreme that they name: `expert_ids`: each row names 2 different experts; among the 16 rows of one index of ep no expert is named more than 8 times, and in the rows of some indices one expert is named exactly 8 times.
All inputs are finite; a program needn't handle non-finite values.
Results may differ from a plain program's by a relative error of at most 0.015.
Values may be sent and summed in bfloat16 or wider, within the bound.
A program may use at most 64 MiB of HBM per device.

v0:
```python
import functools
import math

import jax
import jax.numpy as jnp
from jax import lax
from jax.experimental import pallas as pl
from jax.experimental.pallas import tpu as pltpu
from jax.sharding import PartitionSpec as P

norm_eps = 1e-06
group_eps = 0.00064


def rms_scale(activity, gain):
    widened = activity.astype(jnp.float32)
    scaled = widened * lax.rsqrt(jnp.mean(widened * widened, axis=-1, keepdims=True) + norm_eps)
    return (scaled * gain).astype(jnp.bfloat16)


def low_rank(normed, decay_down, decay_up, decay_base, rate_down, rate_up):
    decay_low = jnp.tanh(jnp.dot(normed, decay_down, preferred_element_type=jnp.float32)).astype(
        jnp.bfloat16
    )
    decay_pre = decay_base + jnp.dot(decay_low, decay_up, preferred_element_type=jnp.float32)
    decays = jnp.exp(-jnp.exp(-jax.nn.softplus(-decay_pre) - 0.5))
    rate_low = jnp.dot(normed, rate_down, preferred_element_type=jnp.float32).astype(jnp.bfloat16)
    rates = jax.nn.sigmoid(jnp.dot(rate_low, rate_up, preferred_element_type=jnp.float32))
    return (decays, rates)


def recurrence(queries, key_rows, value_rows, decays, rates, old_state, head_gain):
    row_count, head_count, _ = old_state.shape
    head_size = queries.shape[1] // head_count
    head_shape = (row_count, head_count, head_size)
    query_heads = queries.astype(jnp.float32).reshape(head_shape)
    key_heads = key_rows.astype(jnp.float32).reshape(head_shape)
    value_heads = value_rows.astype(jnp.float32).reshape(head_shape)
    decay_heads = decays.reshape(head_shape)
    rate_heads = rates.reshape(head_shape)
    unit_keys = key_heads * lax.rsqrt(jnp.sum(key_heads * key_heads, axis=-1, keepdims=True) + 1.0)
    state_grid = old_state.reshape(row_count, head_count, head_size, head_size)
    removed = jnp.sum(state_grid * unit_keys[:, :, None, :], axis=-1)
    updated = (
        state_grid * decay_heads[:, :, None, :]
        - removed[:, :, :, None] * (unit_keys * rate_heads)[:, :, None, :]
        + value_heads[:, :, :, None] * key_heads[:, :, None, :]
    )
    readout = jnp.sum(updated * query_heads[:, :, None, :], axis=-1)
    centred = readout - jnp.mean(readout, axis=-1, keepdims=True)
    spread = jnp.mean(centred * centred, axis=-1, keepdims=True)
    scaled = centred * lax.rsqrt(spread + group_eps) * head_gain.reshape(head_count, head_size)
    return (
        updated.reshape(row_count, head_count, head_size * head_size),
        scaled.reshape(row_count, head_count * head_size).astype(jnp.bfloat16),
    )


def gathered_body(
    tokens,
    head_state,
    mixer_gain,
    w_query,
    w_key,
    w_value,
    decay_down,
    decay_up,
    decay_base,
    rate_down,
    rate_up,
    head_gain,
    w_out,
    expert_gain,
    expert_ids,
    route_weight,
    w_gate,
    w_up,
    w_down,
):
    seq_rows, width = tokens.shape
    local_cols = w_query.shape[1]
    head_lane = lax.axis_index("tp")
    normed = rms_scale(tokens, mixer_gain)
    pieces = (
        lax.all_gather(w_query, "ep", axis=0, tiled=True),
        lax.all_gather(w_key, "ep", axis=0, tiled=True),
        lax.all_gather(w_value, "ep", axis=0, tiled=True),
    )
    projected = tuple(
        (
            jnp.dot(normed, weight_piece, preferred_element_type=jnp.float32)
            for weight_piece in pieces
        )
    )
    queries, key_rows, value_rows = (member.astype(jnp.bfloat16) for member in projected)
    col_offset = head_lane * local_cols
    decays, rates = low_rank(
        normed,
        decay_down,
        lax.dynamic_slice_in_dim(decay_up, col_offset, local_cols, 1),
        decay_base,
        rate_down,
        lax.dynamic_slice_in_dim(rate_up, col_offset, local_cols, 1),
    )
    next_state, head_out = recurrence(
        queries, key_rows, value_rows, decays, rates, head_state, head_gain
    )
    partial_out = jnp.dot(
        head_out,
        lax.all_gather(w_out, "ep", axis=1, tiled=True),
        preferred_element_type=jnp.float32,
    )
    mixed_out = lax.psum(partial_out.astype(jnp.bfloat16), "tp").astype(jnp.float32)
    residual = (tokens.astype(jnp.float32) + mixed_out).astype(jnp.bfloat16)
    expert_in = rms_scale(residual, expert_gain)
    experts = lax.axis_size("ep")
    top_count = expert_ids.shape[1]
    slot_count = max(1, 2 * seq_rows * top_count // experts)
    slot_total = experts * slot_count
    flat_ids = expert_ids.reshape(-1)
    matches = (flat_ids[:, None] == jnp.arange(experts, dtype=jnp.int32)[None, :]).astype(jnp.int32)
    slot_rank = jnp.sum((jnp.cumsum(matches, axis=0) - 1) * matches, axis=1)
    slot_ids = (flat_ids * slot_count + slot_rank).reshape(seq_rows, top_count)
    slot_match = (
        slot_ids[:, :, None] == jnp.arange(slot_total, dtype=jnp.int32)[None, None, :]
    ).astype(jnp.float32)
    picker = jnp.sum(slot_match, axis=1).astype(jnp.bfloat16)
    outbound = jnp.einsum("ts,td->sd", picker, expert_in, preferred_element_type=jnp.float32)
    outbound = outbound.astype(jnp.bfloat16).reshape(experts, slot_count, expert_in.shape[1])
    gate_local, up_local, down_local = (w_gate[0], w_up[0], w_down[0])
    arrived = lax.all_to_all(outbound, "ep", split_axis=0, concat_axis=0, tiled=True)
    sources, held, _ = arrived.shape
    flat_rows = arrived.reshape(sources * held, width)
    gate_act = jnp.dot(flat_rows, gate_local, preferred_element_type=jnp.float32)
    up_act = jnp.dot(flat_rows, up_local, preferred_element_type=jnp.float32)
    hidden = (jax.nn.silu(gate_act) * up_act).astype(jnp.bfloat16)
    partial_rows = jnp.dot(hidden, down_local, preferred_element_type=jnp.float32).reshape(
        sources, held, width
    )
    reduced = lax.psum_scatter(
        partial_rows.astype(jnp.bfloat16), "tp", scatter_dimension=2, tiled=True
    )
    returned = lax.all_to_all(reduced, "ep", split_axis=0, concat_axis=0, tiled=True)
    shares = route_weight / jnp.sum(route_weight, axis=1, keepdims=True)
    combine = jnp.sum(slot_match * shares[:, :, None], axis=1)
    routed = jnp.dot(
        combine,
        returned.reshape(slot_total, -1).astype(jnp.float32),
        precision=lax.Precision.HIGHEST,
    )
    own_cols = routed.shape[1]
    kept = lax.dynamic_slice_in_dim(residual, head_lane * own_cols, own_cols, 1)
    layer_out = (kept.astype(jnp.float32) + routed).astype(jnp.bfloat16)
    return (layer_out, next_state)


f32, bf16 = jnp.float32, jnp.bfloat16


def mm(a, b):
    return jnp.dot(a, b, preferred_element_type=f32)


def split(x):
    top = x.astype(bf16)
    return top, (x - top.astype(f32)).astype(bf16)


def mm_split(x, b):
    top, rest = split(x)
    return mm(top, b) + mm(rest, b)


def ones_where(shape, test):
    rows = lax.broadcasted_iota(jnp.int32, shape, 0)
    cols = lax.broadcasted_iota(jnp.int32, shape, 1)
    return jnp.where(test(rows, cols), 1.0, 0.0).astype(bf16)


def repeat_lanes(x, width):
    return jnp.concatenate([x] * (width // x.shape[1]), axis=1)


def mm_last(a, b):
    return lax.dot_general(a, b, (((1,), (1,)), ((), ())), preferred_element_type=f32)


IN_NAMES = (
    "tok", "ids", "wts", "gain", "ddT", "rdT", "dbase", "dup", "rup", "wq", "wk", "wv",
    "state", "hgain", "wout", "egain", "wg", "wu", "wd",
)


def layer_kernel(n, m, *refs):
    hbm = dict(zip(IN_NAMES, refs))
    refs = refs[len(IN_NAMES) :]
    out, nxt = refs[:2]
    v = dict(zip(IN_NAMES[:-3], refs[2:]))
    refs = refs[2 + len(IN_NAMES) - 3 :]
    (next_v, store_sem, wg2, wu2, wd2, x_r, id_r, q_s, q_r, ho_s, ho_r, p_s, p_r, res_s, own_r, sl_s, sl_r,
     ret_s, ret_r, lsem, w_ss, w_rs, x_ss, x_rs, id_ss, id_rs, q_ss, q_rs, ho_ss, ho_rs, p_ss, p_rs,
     sl_ss, sl_rs, own_ss, own_rs, ret_ss, ret_rs) = refs
    me, lane = lax.axis_index("ep"), lax.axis_index("tp")
    half, core = lane // 2, lax.rem(lane, 2)
    halves = m // 2
    tok, gain = v["tok"], v["gain"]
    B, D = tok.shape
    Ke, C = v["wq"].shape
    heads, wide = v["state"].shape[1:]
    hs = C // heads
    G = n // m
    cap = ret_s.shape[2]
    top = v["ids"].shape[0]
    own_cols = D // m
    F = hbm["wg"].shape[2]

    def remote(src, dst, ss, rs, e, t):
        return pltpu.make_async_remote_copy(
            src_ref=src, dst_ref=dst, send_sem=ss, recv_sem=rs,
            device_id=(e, t), device_id_type=pl.DeviceIdType.MESH,
        )

    barrier = pltpu.get_barrier_semaphore()
    for ke in range(n):
        for kt in range(m):
            if ke or kt:
                pl.semaphore_signal(
                    barrier, inc=1, device_id=(lax.rem(me + ke, n), lax.rem(lane + kt, m)),
                    device_id_type=pl.DeviceIdType.MESH,
                )
    loads = {}
    for i, name in enumerate(IN_NAMES[:-3]):
        loads[name] = pltpu.make_async_copy(hbm[name], v[name], lsem.at[i])
    my_hidden = pl.ds(pl.multiple_of(core * F, F), F)
    spots = (wg2.at[:, my_hidden], wu2.at[:, my_hidden], wd2.at[my_hidden])
    for i, name in enumerate(IN_NAMES[-3:]):
        loads[name] = pltpu.make_async_copy(hbm[name].at[0], spots[i], lsem.at[len(IN_NAMES) - 3 + i])
    for name in IN_NAMES:
        loads[name].start()

    def partner(i, k, count):
        if count & (count - 1):
            return lax.rem(i + k, count)
        for bit in range(count.bit_length() - 1):
            if k >> bit & 1:
                i = i + (1 << bit) * (1 - 2 * (i // (1 << bit) % 2))
        return i

    offsets = list(range(n - 1, 0, -1))
    ep_peers = [(k, partner(me, k, n), lane) for k in offsets]
    tp_peers = [(k, me, lax.rem(lane + k, m)) for k in range(m - 1, 0, -1)]
    slot_peers = [
        ((k, j), partner(me, k, n), lax.rem(lane + 2 * j, m))
        for k in range(n - 1, -1, -1) for j in range(halves - 1, -1, -1) if k or j
    ]
    pending = []

    def send(peers, src_of, dst, ss, rs):
        copies = [remote(src_of(e, t), dst, ss.at[k], rs.at[k], e, t) for k, e, t in peers]
        for c in copies:
            c.start()
        pending.extend(copies)
        return copies

    def arrive(copies):
        for c in copies:
            c.wait_recv()

    def cols_of(ref, index, size):
        return ref[:, pl.ds(pl.multiple_of(index * size, size), size)]

    loads["tok"].wait()
    loads["ids"].wait()
    pl.semaphore_wait(barrier, n * m - 1)
    cx = send(
        ep_peers, lambda e, t: tok.at[:, pl.ds(pl.multiple_of(e * Ke, Ke), Ke)], x_r.at[me], x_ss, x_rs
    )
    cid = send(ep_peers, lambda e, t: v["ids"], id_r.at[me], id_ss, id_rs)
    x_r[me] = cols_of(tok, me, Ke)
    id_r[me] = v["ids"][...]

    for name in IN_NAMES[2:-3]:
        loads[name].wait()
    wide_tok = tok[...].astype(f32)
    scale = lax.rsqrt(jnp.mean(wide_tok * wide_tok, axis=-1, keepdims=True) + norm_eps)
    normed = (wide_tok * scale * gain[...]).astype(bf16)
    decay_low = jnp.tanh(mm_last(normed, v["ddT"][...])).astype(bf16)
    decay_pre = v["dbase"][...] + mm(decay_low, cols_of(v["dup"], lane, C))
    decays = jnp.exp(-(math.exp(-0.5) / (1.0 + jnp.exp(-decay_pre))))
    rate_low = mm_last(normed, v["rdT"][...]).astype(bf16)
    rates = 1.0 / (1.0 + jnp.exp(-mm(rate_low, cols_of(v["rup"], lane, C))))

    R = B * heads
    rep = ones_where((R, B), lambda r, c: r // heads == c)
    rep_t = ones_where((B, R), lambda r, c: c // heads == r)
    head_mask = ones_where((R, C), lambda r, c: c // hs == r % heads).astype(f32)
    fold2 = ones_where((C, 2 * hs), lambda r, c: r % hs == c % hs)
    unfold = ones_where((hs, C), lambda r, c: c % hs == r)
    summing = ones_where((wide, hs), lambda r, c: r // hs == c)
    spreading = ones_where((hs, wide), lambda r, c: c // hs == r)

    def spread(x):
        return mm((mm(rep, x) * head_mask).astype(bf16), fold2)

    def spread_split(x):
        top_part, rest = split(x)
        return spread(top_part) + spread(rest)

    decay_rows = spread_split(decays)
    rate_rows = spread_split(rates)
    gain_rows = spread_split(jnp.broadcast_to(v["hgain"][...], (B, C)))[:, :hs]

    def choice(ids, row_expert, row_slot, same):
        named = functools.reduce(jnp.logical_or, [ids[k : k + 1] == row_expert for k in range(top)])
        hit = jnp.where(jnp.logical_and(named, same), 1.0, 0.0)
        width = hit.shape[1]
        earlier = ones_where((width, width), lambda r, c: jnp.logical_and(r < c, r // B == c // B))
        rank = mm(hit.astype(bf16), earlier)
        return jnp.where(rank == row_slot, hit, 0.0)

    shape = (n * cap, B)
    row = lax.broadcasted_iota(jnp.int32, shape, 0)
    ids = v["ids"][...]
    wts = v["wts"][...]
    shares = wts / jnp.sum(wts, axis=0, keepdims=True)
    share_of = functools.reduce(
        jnp.add, [jnp.where(ids[k : k + 1] == row // cap, shares[k : k + 1], 0.0) for k in range(top)]
    )
    taken = choice(ids, row // cap, (row % cap).astype(f32), row >= 0) * share_of
    eye = ones_where((B, B), lambda r, c: r == c)
    combine = [mm_last(eye, part).astype(bf16) for part in split(taken)]

    arrive(cx)
    rows = x_r[...].reshape(n * B, Ke)
    scaled_rows = (rows.astype(f32) * cols_of(gain, me, Ke)).astype(bf16)
    for i, w in enumerate(("wq", "wk", "wv")):
        q_s[:, :, i * C : (i + 1) * C] = mm(scaled_rows, v[w][...]).astype(bf16).reshape(n, B, C)
    cq = send(ep_peers, lambda e, t: q_s.at[e], q_r.at[me], q_ss, q_rs)
    q_r[me] = q_s[me]

    arrive(cid)
    shape = (n * G * cap, G * B)
    row = lax.broadcasted_iota(jnp.int32, shape, 0)
    col = lax.broadcasted_iota(jnp.int32, shape, 1)
    group_ids = jnp.concatenate([id_r[lane * G + g] for g in range(G)], axis=1)
    picker = choice(
        group_ids, row // (G * cap), (row % cap).astype(f32), row // cap % G == col // B
    ).astype(bf16)

    S = v["state"][...].reshape(R, wide)
    arrive(cq)
    mate = me, half * 2 + (1 - core)
    cw = [
        remote(hbm[name].at[0], spots[i], w_ss.at[i], w_rs.at[i], *mate)
        for i, name in enumerate(IN_NAMES[-3:])
    ]
    for c in cw:
        c.start()
    pending.extend(cw)
    qkv = (jnp.sum(q_r[...].astype(f32), axis=0) * scale).astype(bf16)
    q_rows, k_rows = spread(qkv[:, :C]), spread(qkv[:, C : 2 * C])
    v_rows = spread(qkv[:, 2 * C :])[:, :hs]
    unit = k_rows * lax.rsqrt(jnp.sum(k_rows * k_rows, axis=-1, keepdims=True) * 0.5 + 1.0)
    both = jnp.concatenate(
        [(S * repeat_lanes(x, wide)).astype(bf16) for x in (unit, decay_rows * q_rows)], axis=0
    )
    both = mm(both, summing)
    removed, decayed_read = both[:R], both[R:]
    unit_rates = unit * rate_rows
    unit_read = jnp.sum(unit_rates * q_rows, axis=-1, keepdims=True) * 0.5
    key_read = jnp.sum(k_rows * q_rows, axis=-1, keepdims=True) * 0.5
    readout = decayed_read - removed * unit_read + v_rows * key_read
    centred = readout - jnp.mean(readout, axis=-1, keepdims=True)
    spread_of = jnp.mean(centred * centred, axis=-1, keepdims=True)
    ho_rows = (centred * lax.rsqrt(spread_of + group_eps) * gain_rows).astype(bf16)
    ho = mm(rep_t, (mm(ho_rows, unfold) * head_mask).astype(bf16)).astype(bf16)
    ho_s[...] = ho
    cho = send(ep_peers, lambda e, t: ho_s, ho_r.at[me], ho_ss, ho_rs)
    ho_r[me] = ho
    updated = (
        S * repeat_lanes(decay_rows, wide)
        - mm_split(removed, spreading) * repeat_lanes(unit_rates, wide)
        + mm(v_rows.astype(bf16), spreading) * repeat_lanes(k_rows, wide)
    )
    next_v[...] = updated.reshape(B, heads, wide)
    store = pltpu.make_async_copy(next_v, nxt, store_sem)
    store.start()

    arrive(cho)
    p_s[...] = mm(ho_r[...].reshape(n * B, C), v["wout"][...]).astype(bf16).reshape(m, G * B, Ke)
    cp = send(tp_peers, lambda e, t: p_s.at[t], p_r.at[lane], p_ss, p_rs)
    p_r[lane] = p_s[lane]
    base = x_r[pl.ds(lane * G, G)].astype(f32).reshape(G * B, Ke)
    arrive(cp)
    res = (base + jnp.sum(p_r[...].astype(f32), axis=0)).astype(bf16)
    sl_s[...] = mm(picker, res).astype(bf16).reshape(n, G * cap, Ke)
    csl = send(slot_peers, lambda e, t: sl_s.at[e], sl_r.at[half, me], sl_ss, sl_rs)
    sl_r[half, me] = sl_s[me]
    res_s[...] = res.reshape(G, B, Ke)
    holder = me // G

    def own_copy(g):
        return remote(
            res_s.at[g], own_r.at[lax.rem(me, G)], own_ss.at[g], own_rs.at[lax.rem(me, G)], lane * G + g, holder
        )

    for g in range(G):
        @pl.when(lane * G + g != me)
        def _():
            own_copy(g).start()

        @pl.when(lane * G + g == me)
        def _():
            own_r[g] = res_s[g]

    for name in IN_NAMES[-3:]:
        loads[name].wait()
    arrive(cw)
    arrive(csl)
    raw = jnp.concatenate(
        [sl_r[:, e].reshape(halves * G * cap, Ke) for e in range(n)], axis=1
    ).astype(f32)
    row_scale = lax.rsqrt(jnp.mean(raw * raw, axis=-1, keepdims=True) + norm_eps)
    xs = (raw * row_scale * v["egain"][...]).astype(bf16)
    gate = mm(xs, wg2[...])
    hidden = (gate / (1.0 + jnp.exp(-gate)) * mm(xs, wu2[...])).astype(bf16)
    y = mm(hidden, wd2[...])
    blocks = [(p, g) for p in range(halves) for g in range(G)]

    def owner(p, g):
        return (2 * p + core) * G + g

    def ret_copy(p, g, t):
        return remote(
            ret_s.at[p * G + g, t], ret_r.at[half, me], ret_ss.at[p * G + g, t], ret_rs.at[half, me],
            owner(p, g), t,
        )

    def not_here(p, g, t):
        return jnp.logical_or(owner(p, g) != me, t != lane)

    for p, g in blocks:
        first = (p * G + g) * cap
        for t in range(m):
            ret_s[p * G + g, t] = y[first : first + cap, t * own_cols : (t + 1) * own_cols].astype(bf16)

            @pl.when(not_here(p, g, t))
            def _():
                ret_copy(p, g, t).start()

        @pl.when(owner(p, g) == me)
        def _():
            ret_r[half, me] = ret_s[p * G + g, lane]

    for g in range(G):
        @pl.when(lane * G + g != me)
        def _():
            remote(res_s.at[g], own_r.at[g], own_ss.at[g], own_rs.at[g], lane * G + g, holder).wait_recv()

    for e in range(n):
        for p in range(halves):
            source = 2 * p + lax.rem(holder, 2)

            @pl.when(jnp.logical_or(e != me, source != lane))
            def _():
                remote(
                    ret_s.at[0, 0], ret_r.at[p, e], ret_ss.at[0, 0], ret_rs.at[p, e], e, source
                ).wait_recv()

    returned = jnp.sum(ret_r[...].astype(f32), axis=0).reshape(n * cap, own_cols).astype(bf16)
    routed = mm(combine[0], returned) + mm(combine[1], returned)
    own = jnp.concatenate([own_r[i] for i in range(G)], axis=1).astype(f32)
    out[...] = (own + routed).astype(bf16)

    for g in range(G):
        @pl.when(lane * G + g != me)
        def _():
            own_copy(g).wait_send()

    for p, g in blocks:
        for t in range(m):
            @pl.when(not_here(p, g, t))
            def _():
                ret_copy(p, g, t).wait_send()

    for c in pending:
        c.wait_send()
    store.wait()


def deliver_kernel(small, large, small_out, large_out, small_v, large_v, sems):
    pieces = sems.shape[1] - 1
    step = large.shape[0] // pieces
    moves = [(small, small_v, small_out)] + [
        tuple(ref.at[pl.ds(i * step, step)] for ref in (large, large_v, large_out)) for i in range(pieces)
    ]
    reads = [pltpu.make_async_copy(a, b, sems.at[0, i]) for i, (a, b, _) in enumerate(moves)]
    writes = [pltpu.make_async_copy(b, c, sems.at[1, i]) for i, (_, b, c) in enumerate(moves)]
    for read in reads:
        read.start()
    for read, write in zip(reads, writes):
        read.wait()
        write.start()
    for write in writes:
        write.wait()


def body(n, m, *args):
    (tokens, head_state, mixer_gain, w_query, w_key, w_value, decay_down, decay_up, decay_base,
     rate_down, rate_up, head_gain, w_out, expert_gain, expert_ids, route_weight, w_gate, w_up, w_down) = args
    B, D = tokens.shape
    Ke, C = w_query.shape
    F = w_gate.shape[2]
    top_count = expert_ids.shape[1]
    cap = max(1, 2 * B * top_count // n)
    if Ke % 128 or C % 128 or F % 128 or (D // m) % 128 or n % m or m % 2 or cap % 8 or B % 16:
        return gathered_body(*args)
    G, own_cols, halves = n // m, D // m, m // 2
    arrays = (
        tokens, expert_ids.T, route_weight.T, mixer_gain[None], decay_down.T, rate_down.T,
        decay_base[None], decay_up, rate_up, w_query, w_key, w_value, head_state,
        head_gain[None], w_out, expert_gain[None], w_gate, w_up, w_down,
    )
    V = pltpu.VMEM
    dma = pltpu.SemaphoreType.DMA
    scratch = [V(a.shape, a.dtype) for a in arrays[:-3]] + [
        V(head_state.shape, f32), dma(()),
        V((D, 2 * F), bf16), V((D, 2 * F), bf16), V((2 * F, D), bf16),
        V((n, B, Ke), bf16), V((n, top_count, B), jnp.int32),
        V((n, B, 3 * C), bf16), V((n, B, 3 * C), bf16),
        V((B, C), bf16), V((n, B, C), bf16),
        V((m, G * B, Ke), bf16), V((m, G * B, Ke), bf16),
        V((G, B, Ke), bf16), V((G, B, Ke), bf16),
        V((n, G * cap, Ke), bf16), V((halves, n, G * cap, Ke), bf16),
        V((halves * G, m, cap, own_cols), bf16), V((halves, n, cap, own_cols), bf16),
        dma((len(arrays),)), dma((3,)), dma((3,)),
        dma((n,)), dma((n,)), dma((n,)), dma((n,)), dma((n,)), dma((n,)), dma((n,)), dma((n,)),
        dma((m,)), dma((m,)), dma((n, halves)), dma((n, halves)),
        dma((G,)), dma((G,)), dma((halves * G, m)), dma((halves, n)),
    ]
    vm = pl.BlockSpec(memory_space=pltpu.VMEM)
    hbm = pl.BlockSpec(memory_space=pltpu.HBM)
    results = (
        jax.ShapeDtypeStruct((B, own_cols), bf16),
        jax.ShapeDtypeStruct(head_state.shape, f32),
    )
    made = pl.pallas_call(
        functools.partial(layer_kernel, n, m),
        out_shape=results,
        in_specs=[hbm] * len(arrays),
        out_specs=(vm, hbm),
        scratch_shapes=scratch,
        compiler_params=pltpu.CompilerParams(
            collective_id=0, has_side_effects=True, vmem_limit_bytes=67_043_328
        ),
    )(*arrays)
    return pl.pallas_call(
        deliver_kernel,
        out_shape=results,
        in_specs=[hbm, hbm],
        out_specs=(hbm, hbm),
        scratch_shapes=[V(a.shape, a.dtype) for a in results] + [dma((2, 1 + math.gcd(B, 4)))],
        compiler_params=pltpu.CompilerParams(vmem_limit_bytes=67_043_328),
    )(*made)


def solution(mesh):
    return jax.shard_map(
        functools.partial(body, mesh.shape["ep"], mesh.shape["tp"]),
        mesh=mesh,
        in_specs=(
            P("ep", None),
            P("ep", "tp", None),
            P(),
            P("ep", "tp"),
            P("ep", "tp"),
            P("ep", "tp"),
            P(),
            P(),
            P("tp"),
            P(),
            P(),
            P("tp"),
            P("tp", "ep"),
            P(),
            P("ep", None),
            P("ep", None),
            P("ep", None, "tp"),
            P("ep", None, "tp"),
            P("ep", "tp", None),
        ),
        out_specs=(P("ep", "tp"), P("ep", "tp", None)),
        check_vma=False,
    )
```

profile of v0, /device:TPU:0, one launch (start us, length us, event | category | flops | bytes accessed | tf_op | source)
XLA Modules:
  0.0 40.6 jit_solution(12602768597558226584)
XLA Ops:
  0.6 37.9 %shard_map.194 = (bf16[16,512]{1,0:T(8,128)(2,1)}, f32[16,4,4096]{2,1,0:T(4,128)}) custom-call(bf16[16,2048]{1,0:T(8,128)(2,1)} %refs_0_.1, s32[2,16]{1,0:T(2,128)} %bitcast.12, f32[2,16]{1,0:T(2,128)} %bitcast.13, f32[1,2048]{1,0:T(1,128)} %bitcast.10, bf16[64,2048]{1,0:T(8,128)(2,1)} %bitcast.8, bf16[64,2048]{1,0:T(8,128)(2,1)} %bitcast.9, ...), custom_call_target="tpu_custom_call" | custom-call | tf_op jit(solution)/shard_map/pallas_call | solution.py:547
  38.6 2.0 %shard_map.195 = (bf16[16,512]{1,0:T(8,128)(2,1)}, f32[16,4,4096]{2,1,0:T(4,128)}) custom-call(bf16[16,512]{1,0:T(8,128)(2,1)} %get-tuple-element.4.small, f32[16,4,4096]{2,1,0:T(4,128)} %get-tuple-element.5.large), custom_call_target="tpu_custom_call" | custom-call | tf_op jit(solution)/shard_map/pallas_call | solution.py:557
where the time goes:
time: 40.8 us; the launch traced here: 40.6 us
  Pallas kernels  39.9 us (98%)
  between operations  0.65 us (2%)
    pallas_call x1, Pallas kernels, body(): pl.pallas_call(functools.partial(layer_kernel, n, m), out_shape=results,...  37.9 us
    pallas_call x1, Pallas kernels, body(): pl.pallas_call(deliver_kernel, out_shape=results, in_specs=[hbm, hbm], ou...  2.02 us

commit v1 on v0

--- a/solution.py
+++ b/solution.py
@@ -197,7 +197,7 @@
     out, nxt = refs[:2]
     v = dict(zip(IN_NAMES[:-3], refs[2:]))
     refs = refs[2 + len(IN_NAMES) - 3 :]
-    (next_v, store_sem, wg2, wu2, wd2, x_r, id_r, q_s, q_r, ho_s, ho_r, p_s, p_r, res_s, own_r, sl_s, sl_r,
+    (wg2, wu2, wd2, x_r, id_r, q_s, q_r, ho_s, ho_r, p_s, p_r, res_s, own_r, sl_s, sl_r,
      ret_s, ret_r, lsem, w_ss, w_rs, x_ss, x_rs, id_ss, id_rs, q_ss, q_rs, ho_ss, ho_rs, p_ss, p_rs,
      sl_ss, sl_rs, own_ss, own_rs, ret_ss, ret_rs) = refs
     me, lane = lax.axis_index("ep"), lax.axis_index("tp")
@@ -382,9 +382,7 @@
         - mm_split(removed, spreading) * repeat_lanes(unit_rates, wide)
         + mm(v_rows.astype(bf16), spreading) * repeat_lanes(k_rows, wide)
     )
-    next_v[...] = updated.reshape(B, heads, wide)
-    store = pltpu.make_async_copy(next_v, nxt, store_sem)
-    store.start()
+    nxt[...] = updated.reshape(B, heads, wide)
 
     arrive(cho)
     p_s[...] = mm(ho_r[...].reshape(n * B, C), v["wout"][...]).astype(bf16).reshape(m, G * B, Ke)
@@ -485,21 +483,16 @@
 
     for c in pending:
         c.wait_send()
-    store.wait()
-
-
-def deliver_kernel(small, large, small_out, large_out, small_v, large_v, sems):
-    pieces = sems.shape[1] - 1
+
+
+def deliver_kernel(small, large, small_out, large_out, sems):
+    pieces = sems.shape[0] - 1
     step = large.shape[0] // pieces
-    moves = [(small, small_v, small_out)] + [
-        tuple(ref.at[pl.ds(i * step, step)] for ref in (large, large_v, large_out)) for i in range(pieces)
+    moves = [(small, small_out)] + [
+        tuple(ref.at[pl.ds(i * step, step)] for ref in (large, large_out)) for i in range(pieces)
     ]
-    reads = [pltpu.make_async_copy(a, b, sems.at[0, i]) for i, (a, b, _) in enumerate(moves)]
-    writes = [pltpu.make_async_copy(b, c, sems.at[1, i]) for i, (_, b, c) in enumerate(moves)]
-    for read in reads:
-        read.start()
-    for read, write in zip(reads, writes):
-        read.wait()
+    writes = [pltpu.make_async_copy(a, b, sems.at[i]) for i, (a, b) in enumerate(moves)]
+    for write in writes:
         write.start()
     for write in writes:
         write.wait()
@@ -521,10 +514,10 @@
         decay_base[None], decay_up, rate_up, w_query, w_key, w_value, head_state,
         head_gain[None], w_out, expert_gain[None], w_gate, w_up, w_down,
     )
+    arrays = tuple(pltpu.with_memory_space_constraint(a, pltpu.HBM) for a in arrays)
     V = pltpu.VMEM
     dma = pltpu.SemaphoreType.DMA
     scratch = [V(a.shape, a.dtype) for a in arrays[:-3]] + [
-        V(head_state.shape, f32), dma(()),
         V((D, 2 * F), bf16), V((D, 2 * F), bf16), V((2 * F, D), bf16),
         V((n, B, Ke), bf16), V((n, top_count, B), jnp.int32),
         V((n, B, 3 * C), bf16), V((n, B, 3 * C), bf16),
@@ -546,21 +539,21 @@
     )
     made = pl.pallas_call(
         functools.partial(layer_kernel, n, m),
-        out_shape=results,
+        out_shape=tuple(pltpu.VMEM(a.shape, a.dtype) for a in results),
         in_specs=[hbm] * len(arrays),
-        out_specs=(vm, hbm),
+        out_specs=(vm, vm),
         scratch_shapes=scratch,
         compiler_params=pltpu.CompilerParams(
-            collective_id=0, has_side_effects=True, vmem_limit_bytes=67_043_328
+            collective_id=0, has_side_effects=True, vmem_limit_bytes=32 * 1024 * 1024
         ),
     )(*arrays)
     return pl.pallas_call(
         deliver_kernel,
         out_shape=results,
-        in_specs=[hbm, hbm],
+        in_specs=[vm, vm],
         out_specs=(hbm, hbm),
-        scratch_shapes=[V(a.shape, a.dtype) for a in results] + [dma((2, 1 + math.gcd(B, 4)))],
-        compiler_params=pltpu.CompilerParams(vmem_limit_bytes=67_043_328),
+        scratch_shapes=[dma((1 + math.gcd(B, 4),))],
+        compiler_params=pltpu.CompilerParams(vmem_limit_bytes=1024 * 1024),
     )(*made)
 
 

time: 40.8 us -> 39.1 us (0.958)
  Pallas kernels: 39.9 us -> 38.3 us
    pallas_call x2, Pallas kernels: 39.9 us -> 38.3 us  [the longest x1 37.3 us: body(): pl.pallas_call(functools.partial(layer_kernel, n, m), out_shape=tuple((pl...]
where the time goes in v1:
time: 39.1 us; the launch traced here: 39 us
  Pallas kernels  38.3 us (98%)
  between operations  0.65 us (2%)
    pallas_call x1, Pallas kernels, body(): pl.pallas_call(functools.partial(layer_kernel, n, m), out_shape=tuple((pl...  37.3 us
    pallas_call x1, Pallas kernels, body(): pl.pallas_call(deliver_kernel, out_shape=results, in_specs=[vm, vm], out_...  1.01 us

profile of v1, /device:TPU:0, one launch (start us, length us, event | category | flops | bytes accessed | tf_op | source)
XLA Modules:
  0.0 39.0 jit_solution(1343743260482775300)
XLA Ops:
  0.6 37.3 %shard_map.194 = (bf16[16,512]{1,0:T(8,128)(2,1)S(1)}, f32[16,4,4096]{2,1,0:T(4,128)S(1)}) custom-call(bf16[16,2048]{1,0:T(8,128)(2,1)} %refs_0_.1, s32[2,16]{1,0:T(2,128)} %bitcast.12, f32[2,16]{1,0:T(2,128)} %bitcast.13, f32[1,2048]{1,0:T(1,128)} %bitcast.10, bf16[64,2048]{1,0:T(8,128)(2,1)} %bitcast.8, bf16[64,2048]{1,0:T(8,128)(2,1)} %bitcast.9, ...), custom_call_target="tpu_custom_call" | custom-call | tf_op jit(solution)/shard_map/pallas_call | solution.py:540
  38.0 1.0 %shard_map.195 = (bf16[16,512]{1,0:T(8,128)(2,1)}, f32[16,4,4096]{2,1,0:T(4,128)}) custom-call(bf16[16,512]{1,0:T(8,128)(2,1)S(1)} %get-tuple-element.4.small, f32[16,4,4096]{2,1,0:T(4,128)S(1)} %get-tuple-element.5.large), custom_call_target="tpu_custom_call" | custom-call | tf_op jit(solution)/shard_map/pallas_call | solution.py:550

commit v2 on v1

--- a/solution.py
+++ b/solution.py
@@ -191,14 +191,17 @@
 )
 
 
+VMEM_NAMES = IN_NAMES[:14] + ("egain",)
+
+
 def layer_kernel(n, m, *refs):
     hbm = dict(zip(IN_NAMES, refs))
     refs = refs[len(IN_NAMES) :]
     out, nxt = refs[:2]
-    v = dict(zip(IN_NAMES[:-3], refs[2:]))
-    refs = refs[2 + len(IN_NAMES) - 3 :]
-    (wg2, wu2, wd2, x_r, id_r, q_s, q_r, ho_s, ho_r, p_s, p_r, res_s, own_r, sl_s, sl_r,
-     ret_s, ret_r, lsem, w_ss, w_rs, x_ss, x_rs, id_ss, id_rs, q_ss, q_rs, ho_ss, ho_rs, p_ss, p_rs,
+    v = dict(zip(VMEM_NAMES, refs[2:]))
+    refs = refs[2 + len(VMEM_NAMES) :]
+    (wo, wg2, wu2, wd2, x_r, id_r, q_s, q_r, ho_s, ho_r, res_s, own_r, sl_s, sl_r, ret_s, ret_r,
+     lsem, w_ss, w_rs, wo_ss, wo_rs, x_ss, x_rs, id_ss, id_rs, q_ss, q_rs, ho_ss, ho_rs,
      sl_ss, sl_rs, own_ss, own_rs, ret_ss, ret_rs) = refs
     me, lane = lax.axis_index("ep"), lax.axis_index("tp")
     half, core = lane // 2, lax.rem(lane, 2)
@@ -213,6 +216,17 @@
     top = v["ids"].shape[0]
     own_cols = D // m
     F = hbm["wg"].shape[2]
+    Q = n // 4
+
+    def lane_of(group):
+        return lax.rem(group, halves) * 2 + lax.rem(group, m) // halves
+
+    def group_of(x, c, g):
+        return x + halves * c + m * g
+
+    my_groups = [group_of(half, core, g) for g in range(G)]
+    my_lane, my_turn = lane_of(me), me // m
+    mine = lane == my_lane
 
     def remote(src, dst, ss, rs, e, t):
         return pltpu.make_async_remote_copy(
@@ -220,75 +234,80 @@
             device_id=(e, t), device_id_type=pl.DeviceIdType.MESH,
         )
 
+    quarter = me // Q
+    low = quarter < 2
+    near_q, far_q = jnp.where(low, 2, 1), jnp.where(low, 3, 0)
+    own_base = me // (2 * Q) * (2 * Q)
+    near = [near_q * Q + lax.rem(me + 1 + i, Q) for i in range(Q)]
+    far = [far_q * Q + lax.rem(me + 1 + i, Q) for i in range(Q)]
+    close = [own_base + lax.rem(me + k, 2 * Q) for k in range(2 * Q - 1, 0, -1)]
+    ep_peers = far + near + close
+    tp_peers = [lax.rem(lane + k, m) for k in range(m - 1, 0, -1)]
+
+    loads = {}
+    spots = {name: v[name] for name in VMEM_NAMES}
+    my_hidden = pl.ds(pl.multiple_of(core * F, F), F)
+    spots["wout"] = wo.at[lane]
+    spots["wg"], spots["wu"], spots["wd"] = wg2.at[:, my_hidden], wu2.at[:, my_hidden], wd2.at[my_hidden]
+    for i, name in enumerate(IN_NAMES):
+        src = hbm[name]
+        if name in ("dup", "rup"):
+            src = src.at[:, pl.ds(pl.multiple_of(lane * C, C), C)]
+        elif name in ("wg", "wu", "wd"):
+            src = src.at[0]
+        loads[name] = pltpu.make_async_copy(src, spots[name], lsem.at[i])
+    loads["tok"].start()
     barrier = pltpu.get_barrier_semaphore()
-    for ke in range(n):
-        for kt in range(m):
-            if ke or kt:
-                pl.semaphore_signal(
-                    barrier, inc=1, device_id=(lax.rem(me + ke, n), lax.rem(lane + kt, m)),
-                    device_id_type=pl.DeviceIdType.MESH,
-                )
-    loads = {}
-    for i, name in enumerate(IN_NAMES[:-3]):
-        loads[name] = pltpu.make_async_copy(hbm[name], v[name], lsem.at[i])
-    my_hidden = pl.ds(pl.multiple_of(core * F, F), F)
-    spots = (wg2.at[:, my_hidden], wu2.at[:, my_hidden], wd2.at[my_hidden])
-    for i, name in enumerate(IN_NAMES[-3:]):
-        loads[name] = pltpu.make_async_copy(hbm[name].at[0], spots[i], lsem.at[len(IN_NAMES) - 3 + i])
-    for name in IN_NAMES:
+    for e, t in [(e, lane) for e in ep_peers] + [(me, t) for t in tp_peers]:
+        pl.semaphore_signal(barrier, inc=1, device_id=(e, t), device_id_type=pl.DeviceIdType.MESH)
+    for name in IN_NAMES[1:]:
         loads[name].start()
 
-    def partner(i, k, count):
-        if count & (count - 1):
-            return lax.rem(i + k, count)
-        for bit in range(count.bit_length() - 1):
-            if k >> bit & 1:
-                i = i + (1 << bit) * (1 - 2 * (i // (1 << bit) % 2))
-        return i
-
-    offsets = list(range(n - 1, 0, -1))
-    ep_peers = [(k, partner(me, k, n), lane) for k in offsets]
-    tp_peers = [(k, me, lax.rem(lane + k, m)) for k in range(m - 1, 0, -1)]
-    slot_peers = [
-        ((k, j), partner(me, k, n), lax.rem(lane + 2 * j, m))
-        for k in range(n - 1, -1, -1) for j in range(halves - 1, -1, -1) if k or j
-    ]
     pending = []
 
-    def send(peers, src_of, dst, ss, rs):
-        copies = [remote(src_of(e, t), dst, ss.at[k], rs.at[k], e, t) for k, e, t in peers]
+    def start(*copies):
         for c in copies:
             c.start()
         pending.extend(copies)
-        return copies
-
-    def arrive(copies):
-        for c in copies:
-            c.wait_recv()
 
     def cols_of(ref, index, size):
         return ref[:, pl.ds(pl.multiple_of(index * size, size), size)]
 
     loads["tok"].wait()
+    pl.semaphore_wait(barrier, n + m - 2)
+    for i, e in enumerate(ep_peers):
+        start(remote(
+            tok.at[:, pl.ds(pl.multiple_of(e * Ke, Ke), Ke)], x_r.at[me], x_ss.at[i], x_rs.at[me], e, lane
+        ))
+    for i, t in enumerate(tp_peers):
+        start(remote(hbm["wout"], wo.at[lane], wo_ss.at[i], wo_rs.at[lane], me, t))
+    mate = me, half * 2 + (1 - core)
+    cw = [
+        remote(hbm[name].at[0], spots[name], w_ss.at[i], w_rs.at[i], *mate)
+        for i, name in enumerate(IN_NAMES[-3:])
+    ]
+    start(*cw)
+    x_r[me] = cols_of(tok, me, Ke)
     loads["ids"].wait()
-    pl.semaphore_wait(barrier, n * m - 1)
-    cx = send(
-        ep_peers, lambda e, t: tok.at[:, pl.ds(pl.multiple_of(e * Ke, Ke), Ke)], x_r.at[me], x_ss, x_rs
-    )
-    cid = send(ep_peers, lambda e, t: v["ids"], id_r.at[me], id_ss, id_rs)
-    x_r[me] = cols_of(tok, me, Ke)
-    id_r[me] = v["ids"][...]
-
-    for name in IN_NAMES[2:-3]:
-        loads[name].wait()
+    id_copies = [remote(v["ids"], id_r.at[my_turn], id_ss.at[i], id_rs.at[my_turn], e, lane) for i, e in enumerate(ep_peers)]
+
+    @pl.when(mine)
+    def _():
+        for c in id_copies:
+            c.start()
+        id_r[my_turn] = v["ids"][...]
+
+    for name in IN_NAMES[2:]:
+        if name not in ("wout", "wg", "wu", "wd"):
+            loads[name].wait()
     wide_tok = tok[...].astype(f32)
     scale = lax.rsqrt(jnp.mean(wide_tok * wide_tok, axis=-1, keepdims=True) + norm_eps)
     normed = (wide_tok * scale * gain[...]).astype(bf16)
     decay_low = jnp.tanh(mm_last(normed, v["ddT"][...])).astype(bf16)
-    decay_pre = v["dbase"][...] + mm(decay_low, cols_of(v["dup"], lane, C))
+    decay_pre = v["dbase"][...] + mm(decay_low, v["dup"][...])
     decays = jnp.exp(-(math.exp(-0.5) / (1.0 + jnp.exp(-decay_pre))))
     rate_low = mm_last(normed, v["rdT"][...]).astype(bf16)
-    rates = 1.0 / (1.0 + jnp.exp(-mm(rate_low, cols_of(v["rup"], lane, C))))
+    rates = 1.0 / (1.0 + jnp.exp(-mm(rate_low, v["rup"][...])))
 
     R = B * heads
     rep = ones_where((R, B), lambda r, c: r // heads == c)
@@ -310,6 +329,22 @@
     rate_rows = spread_split(rates)
     gain_rows = spread_split(jnp.broadcast_to(v["hgain"][...], (B, C)))[:, :hs]
 
+    def project(first, count, peers):
+        for e in peers:
+            remote(x_r.at[e], x_r.at[e], x_ss.at[0], x_rs.at[e], e, lane).wait_recv()
+        block = pl.ds(pl.multiple_of(first, count), count)
+        rows = x_r[block].reshape(count * B, Ke)
+        scaled_rows = (rows.astype(f32) * cols_of(gain, me, Ke)).astype(bf16)
+        for i, w in enumerate(("wq", "wk", "wv")):
+            q_s[block, :, i * C : (i + 1) * C] = mm(scaled_rows, v[w][...]).astype(bf16).reshape(count, B, C)
+        for e in peers:
+            start(remote(q_s.at[e], q_r.at[me], q_ss.at[e], q_rs.at[me], e, lane))
+
+    project(near_q * Q, Q, near)
+    project(own_base, 2 * Q, close)
+    project(far_q * Q, Q, far)
+    q_r[me] = q_s[me]
+
     def choice(ids, row_expert, row_slot, same):
         named = functools.reduce(jnp.logical_or, [ids[k : k + 1] == row_expert for k in range(top)])
         hit = jnp.where(jnp.logical_and(named, same), 1.0, 0.0)
@@ -330,33 +365,23 @@
     eye = ones_where((B, B), lambda r, c: r == c)
     combine = [mm_last(eye, part).astype(bf16) for part in split(taken)]
 
-    arrive(cx)
-    rows = x_r[...].reshape(n * B, Ke)
-    scaled_rows = (rows.astype(f32) * cols_of(gain, me, Ke)).astype(bf16)
-    for i, w in enumerate(("wq", "wk", "wv")):
-        q_s[:, :, i * C : (i + 1) * C] = mm(scaled_rows, v[w][...]).astype(bf16).reshape(n, B, C)
-    cq = send(ep_peers, lambda e, t: q_s.at[e], q_r.at[me], q_ss, q_rs)
-    q_r[me] = q_s[me]
-
-    arrive(cid)
+    for g in range(G):
+        @pl.when(my_groups[g] != me)
+        def _():
+            remote(id_r.at[g], id_r.at[g], id_ss.at[0], id_rs.at[g], my_groups[g], lane).wait_recv()
+
     shape = (n * G * cap, G * B)
     row = lax.broadcasted_iota(jnp.int32, shape, 0)
     col = lax.broadcasted_iota(jnp.int32, shape, 1)
-    group_ids = jnp.concatenate([id_r[lane * G + g] for g in range(G)], axis=1)
+    group_ids = jnp.concatenate([id_r[g] for g in range(G)], axis=1)
     picker = choice(
         group_ids, row // (G * cap), (row % cap).astype(f32), row // cap % G == col // B
     ).astype(bf16)
+    base = jnp.concatenate([x_r[my_groups[g]] for g in range(G)], axis=0).astype(f32)
 
     S = v["state"][...].reshape(R, wide)
-    arrive(cq)
-    mate = me, half * 2 + (1 - core)
-    cw = [
-        remote(hbm[name].at[0], spots[i], w_ss.at[i], w_rs.at[i], *mate)
-        for i, name in enumerate(IN_NAMES[-3:])
-    ]
-    for c in cw:
-        c.start()
-    pending.extend(cw)
+    for e in close + near + far:
+        remote(q_r.at[e], q_r.at[e], q_ss.at[0], q_rs.at[e], e, lane).wait_recv()
     qkv = (jnp.sum(q_r[...].astype(f32), axis=0) * scale).astype(bf16)
     q_rows, k_rows = spread(qkv[:, :C]), spread(qkv[:, C : 2 * C])
     v_rows = spread(qkv[:, 2 * C :])[:, :hs]
@@ -375,67 +400,104 @@
     ho_rows = (centred * lax.rsqrt(spread_of + group_eps) * gain_rows).astype(bf16)
     ho = mm(rep_t, (mm(ho_rows, unfold) * head_mask).astype(bf16)).astype(bf16)
     ho_s[...] = ho
-    cho = send(ep_peers, lambda e, t: ho_s, ho_r.at[me], ho_ss, ho_rs)
-    ho_r[me] = ho
+
+    def ho_copy(e, i):
+        return remote(ho_s, ho_r.at[my_turn, lane], ho_ss.at[i], ho_rs.at[my_turn, lane], e, my_lane)
+
+    start(*[ho_copy(e, i) for i, e in enumerate(ep_peers)])
+
+    @pl.when(jnp.logical_not(mine))
+    def _():
+        ho_copy(me, n - 1).start()
+
+    @pl.when(mine)
+    def _():
+        ho_r[my_turn, lane] = ho_s[...]
+
     updated = (
         S * repeat_lanes(decay_rows, wide)
         - mm_split(removed, spreading) * repeat_lanes(unit_rates, wide)
         + mm(v_rows.astype(bf16), spreading) * repeat_lanes(k_rows, wide)
     )
     nxt[...] = updated.reshape(B, heads, wide)
-
-    arrive(cho)
-    p_s[...] = mm(ho_r[...].reshape(n * B, C), v["wout"][...]).astype(bf16).reshape(m, G * B, Ke)
-    cp = send(tp_peers, lambda e, t: p_s.at[t], p_r.at[lane], p_ss, p_rs)
-    p_r[lane] = p_s[lane]
-    base = x_r[pl.ds(lane * G, G)].astype(f32).reshape(G * B, Ke)
-    arrive(cp)
-    res = (base + jnp.sum(p_r[...].astype(f32), axis=0)).astype(bf16)
+    loads["wout"].wait()
+    for t in tp_peers:
+        remote(wo.at[t], wo.at[t], wo_ss.at[0], wo_rs.at[t], me, t).wait_recv()
+
+    for g in range(G):
+        for t in range(m):
+            @pl.when(jnp.logical_or(my_groups[g] != me, t != lane))
+            def _():
+                remote(ho_r.at[g, t], ho_r.at[g, t], ho_ss.at[0], ho_rs.at[g, t], my_groups[g], t).wait_recv()
+
+    mixed = functools.reduce(jnp.add, [mm(ho_r[:, t].reshape(G * B, C), wo[t]) for t in range(m)])
+    res = (base + mixed).astype(bf16)
     sl_s[...] = mm(picker, res).astype(bf16).reshape(n, G * cap, Ke)
-    csl = send(slot_peers, lambda e, t: sl_s.at[e], sl_r.at[half, me], sl_ss, sl_rs)
+    slot_peers = [(e, lax.rem(lane + 2 * j, m)) for j in range(halves - 1, -1, -1) for e in ep_peers]
+    slot_peers += [(me, lax.rem(lane + 2 * j, m)) for j in range(halves - 1, 0, -1)]
+    start(*[
+        remote(sl_s.at[e], sl_r.at[half, me], sl_ss.at[i], sl_rs.at[half, me], e, t)
+        for i, (e, t) in enumerate(slot_peers)
+    ])
     sl_r[half, me] = sl_s[me]
     res_s[...] = res.reshape(G, B, Ke)
-    holder = me // G
+    holder, place = me // G, lax.rem(me, G)
 
     def own_copy(g):
         return remote(
-            res_s.at[g], own_r.at[lax.rem(me, G)], own_ss.at[g], own_rs.at[lax.rem(me, G)], lane * G + g, holder
+            res_s.at[g], own_r.at[place], own_ss.at[g], own_rs.at[place], my_groups[g], holder
         )
 
+    def own_here(g):
+        return jnp.logical_and(my_groups[g] == me, holder == lane)
+
     for g in range(G):
-        @pl.when(lane * G + g != me)
+        @pl.when(jnp.logical_not(own_here(g)))
         def _():
             own_copy(g).start()
 
-        @pl.when(lane * G + g == me)
+        @pl.when(own_here(g))
         def _():
-            own_r[g] = res_s[g]
+            own_r[place] = res_s[g]
 
     for name in IN_NAMES[-3:]:
         loads[name].wait()
-    arrive(cw)
-    arrive(csl)
-    raw = jnp.concatenate(
-        [sl_r[:, e].reshape(halves * G * cap, Ke) for e in range(n)], axis=1
-    ).astype(f32)
-    row_scale = lax.rsqrt(jnp.mean(raw * raw, axis=-1, keepdims=True) + norm_eps)
-    xs = (raw * row_scale * v["egain"][...]).astype(bf16)
-    gate = mm(xs, wg2[...])
-    hidden = (gate / (1.0 + jnp.exp(-gate)) * mm(xs, wu2[...])).astype(bf16)
+    for c in cw:
+        c.wait_recv()
+
+    def slots_in(first, count, sources):
+        for p in range(halves):
+            for e in sources:
+                remote(sl_r.at[p, e], sl_r.at[p, e], sl_ss.at[0], sl_rs.at[p, e], e, 2 * p + core).wait_recv()
+        if sources is close:
+            for j in range(1, halves):
+                p = lax.rem(half + j, halves)
+                remote(sl_r.at[p, me], sl_r.at[p, me], sl_ss.at[0], sl_rs.at[p, me], me, 2 * p + core).wait_recv()
+        raw = jnp.concatenate(
+            [sl_r[:, first + e].reshape(halves * G * cap, Ke) for e in range(count)], axis=1
+        ).astype(f32)
+        block = pl.ds(pl.multiple_of(first * Ke, Ke), count * Ke)
+        xs = (raw * v["egain"][:, block]).astype(bf16)
+        return jnp.sum(raw * raw, axis=-1, keepdims=True), mm(xs, wg2[block]), mm(xs, wu2[block])
+
+    parts = [slots_in(own_base, 2 * Q, close)]
+    parts.append(slots_in(near_q * Q, Q, near))
+    parts.append(slots_in(far_q * Q, Q, far))
+    square, gate, up = (functools.reduce(jnp.add, terms) for terms in zip(*parts))
+    row_scale = lax.rsqrt(square / D + norm_eps)
+    gate = gate * row_scale
+    hidden = (gate / (1.0 + jnp.exp(-gate)) * (up * row_scale)).astype(bf16)
     y = mm(hidden, wd2[...])
     blocks = [(p, g) for p in range(halves) for g in range(G)]
-
-    def owner(p, g):
-        return (2 * p + core) * G + g
 
     def ret_copy(p, g, t):
         return remote(
             ret_s.at[p * G + g, t], ret_r.at[half, me], ret_ss.at[p * G + g, t], ret_rs.at[half, me],
-            owner(p, g), t,
+            group_of(p, core, g), t,
         )
 
     def not_here(p, g, t):
-        return jnp.logical_or(owner(p, g) != me, t != lane)
+        return jnp.logical_or(group_of(p, core, g) != me, t != lane)
 
     for p, g in blocks:
         first = (p * G + g) * cap
@@ -446,18 +508,20 @@
             def _():
                 ret_copy(p, g, t).start()
 
-        @pl.when(owner(p, g) == me)
+        @pl.when(group_of(p, core, g) == me)
         def _():
             ret_r[half, me] = ret_s[p * G + g, lane]
 
-    for g in range(G):
-        @pl.when(lane * G + g != me)
+    for i in range(G):
+        source = lane * G + i
+
+        @pl.when(jnp.logical_not(jnp.logical_and(source == me, mine)))
         def _():
-            remote(res_s.at[g], own_r.at[g], own_ss.at[g], own_rs.at[g], lane * G + g, holder).wait_recv()
+            remote(own_r.at[i], own_r.at[i], own_ss.at[0], own_rs.at[i], source, my_lane).wait_recv()
 
     for e in range(n):
         for p in range(halves):
-            source = 2 * p + lax.rem(holder, 2)
+            source = 2 * p + lax.rem(my_lane, 2)
 
             @pl.when(jnp.logical_or(e != me, source != lane))
             def _():
@@ -470,8 +534,17 @@
     own = jnp.concatenate([own_r[i] for i in range(G)], axis=1).astype(f32)
     out[...] = (own + routed).astype(bf16)
 
+    @pl.when(mine)
+    def _():
+        for c in id_copies:
+            c.wait_send()
+
+    @pl.when(jnp.logical_not(mine))
+    def _():
+        ho_copy(me, n - 1).wait_send()
+
     for g in range(G):
-        @pl.when(lane * G + g != me)
+        @pl.when(jnp.logical_not(own_here(g)))
         def _():
             own_copy(g).wait_send()
 
@@ -506,7 +579,7 @@
     F = w_gate.shape[2]
     top_count = expert_ids.shape[1]
     cap = max(1, 2 * B * top_count // n)
-    if Ke % 128 or C % 128 or F % 128 or (D // m) % 128 or n % m or m % 2 or cap % 8 or B % 16:
+    if Ke % 128 or C % 128 or F % 128 or (D // m) % 128 or n % m or n % 4 or m % 2 or cap % 8 or B % 16:
         return gathered_body(*args)
     G, own_cols, halves = n // m, D // m, m // 2
     arrays = (
@@ -517,18 +590,20 @@
     arrays = tuple(pltpu.with_memory_space_constraint(a, pltpu.HBM) for a in arrays)
     V = pltpu.VMEM
     dma = pltpu.SemaphoreType.DMA
-    scratch = [V(a.shape, a.dtype) for a in arrays[:-3]] + [
-        V((D, 2 * F), bf16), V((D, 2 * F), bf16), V((2 * F, D), bf16),
-        V((n, B, Ke), bf16), V((n, top_count, B), jnp.int32),
+    shapes = {name: a.shape for name, a in zip(IN_NAMES, arrays)}
+    shapes["dup"] = shapes["rup"] = (decay_up.shape[0], C)
+    kinds = {name: a.dtype for name, a in zip(IN_NAMES, arrays)}
+    scratch = [V(shapes[name], kinds[name]) for name in VMEM_NAMES] + [
+        V((m, C, Ke), bf16), V((D, 2 * F), bf16), V((D, 2 * F), bf16), V((2 * F, D), bf16),
+        V((n, B, Ke), bf16), V((G, top_count, B), jnp.int32),
         V((n, B, 3 * C), bf16), V((n, B, 3 * C), bf16),
-        V((B, C), bf16), V((n, B, C), bf16),
-        V((m, G * B, Ke), bf16), V((m, G * B, Ke), bf16),
+        V((B, C), bf16), V((G, m, B, C), bf16),
         V((G, B, Ke), bf16), V((G, B, Ke), bf16),
         V((n, G * cap, Ke), bf16), V((halves, n, G * cap, Ke), bf16),
         V((halves * G, m, cap, own_cols), bf16), V((halves, n, cap, own_cols), bf16),
-        dma((len(arrays),)), dma((3,)), dma((3,)),
-        dma((n,)), dma((n,)), dma((n,)), dma((n,)), dma((n,)), dma((n,)), dma((n,)), dma((n,)),
-        dma((m,)), dma((m,)), dma((n, halves)), dma((n, halves)),
+        dma((len(arrays),)), dma((3,)), dma((3,)), dma((m,)), dma((m,)),
+        dma((n,)), dma((n,)), dma((n,)), dma((G,)), dma((n,)), dma((n,)), dma((n,)), dma((G, m)),
+        dma((n * halves,)), dma((halves, n)),
         dma((G,)), dma((G,)), dma((halves * G, m)), dma((halves, n)),
     ]
     vm = pl.BlockSpec(memory_space=pltpu.VMEM)

time: 39.1 us -> 34.7 us (0.89)
  Pallas kernels: 38.3 us -> 33.9 us
    pallas_call x1, Pallas kernels: 37.3 us -> 32.9 us  [body(): pl.pallas_call(functools.partial(layer_kernel, n, m), out_shape=tuple((pl...]
where the time goes in v2:
time: 34.7 us; the launch traced here: 34.5 us
  Pallas kernels  33.9 us (98%)
  between operations  0.65 us (2%)
    pallas_call x1, Pallas kernels, body(): pl.pallas_call(functools.partial(layer_kernel, n, m), out_shape=tuple((pl...  32.9 us
    pallas_call x1, Pallas kernels, body(): pl.pallas_call(deliver_kernel, out_shape=results, in_specs=[vm, vm], out_...  1.01 us

profile of v2, /device:TPU:0, one launch (start us, length us, event | category | flops | bytes accessed | tf_op | source)
XLA Modules:
  0.0 34.5 jit_solution(817407287918109507)
XLA Ops:
  0.6 32.9 %shard_map.194 = (bf16[16,512]{1,0:T(8,128)(2,1)S(1)}, f32[16,4,4096]{2,1,0:T(4,128)S(1)}) custom-call(bf16[16,2048]{1,0:T(8,128)(2,1)} %refs_0_.1, s32[2,16]{1,0:T(2,128)} %bitcast.12, f32[2,16]{1,0:T(2,128)} %bitcast.13, f32[1,2048]{1,0:T(1,128)} %bitcast.10, bf16[64,2048]{1,0:T(8,128)(2,1)} %bitcast.8, bf16[64,2048]{1,0:T(8,128)(2,1)} %bitcast.9, ...), custom_call_target="tpu_custom_call" | custom-call | tf_op jit(solution)/shard_map/pallas_call | solution.py:615
  33.5 1.0 %shard_map.195 = (bf16[16,512]{1,0:T(8,128)(2,1)}, f32[16,4,4096]{2,1,0:T(4,128)}) custom-call(bf16[16,512]{1,0:T(8,128)(2,1)S(1)} %get-tuple-element.4.small, f32[16,4,4096]{2,1,0:T(4,128)S(1)} %get-tuple-element.5.large), custom_call_target="tpu_custom_call" | custom-call | tf_op jit(solution)/shard_map/pallas_call | solution.py:625
